TPU v7x, 32 devices: a whole 2x2x4 slice. The times are simulated.
32 devices in a mesh: sp: 16 (over z, y, x), tp: 2 (over core).
Axes of the slice: x: 2, y: 2, z: 4, core: 2. Of those that a mesh axis runs over, the one named last changes fastest.
Arguments:
- tokens: bfloat16 [4096, 2048], P('sp', 'tp'), may hold values from -6 to 6
- norm_gain: float32 [2048], replicated, may hold values from 0.1 to 1.9
- query_weight: bfloat16 [1024, 2048], P('tp'), may hold values from -0.125 to 0.125
- key_weight: bfloat16 [1024, 2048], P('tp'), may hold values from -0.125 to 0.125
- value_weight: bfloat16 [1024, 2048], P('tp'), may hold values from -0.125 to 0.125
- pool_weight: bfloat16 [1024, 2048], P('tp'), may hold values from -0.125 to 0.125
- query_gain: float32 [64], replicated, may hold values from 0.6 to 6
- key_gain: float32 [64], replicated, may hold values from 0.6 to 6
- cum_gate: float32 [4096, 16], P('sp', 'tp'), as said below
- out_pool_weight: bfloat16 [1024, 2048], P(None, 'tp'), may hold values from -0.1875 to 0.1875
- out_attn_weight: bfloat16 [1024, 2048], P(None, 'tp'), may hold values from -0.1875 to 0.1875
Outputs:
- mixed: bfloat16 [4096, 2048], P('sp', 'tp')
Inputs may be any that keep to these rules, and one draw needn't show every extreme that they name: `cum_gate`: in each head the values never rise along the positions.
All inputs are finite; a program needn't handle non-finite values.
Results may differ from a plain program's by a relative error of at most 0.005.
The roundings to bfloat16 on the way count: a program that leaves them out, or rounds other values in their place, can miss the bound.
Values may be sent and summed in bfloat16 or wider, within the bound.
A program may use at most 128 MiB of HBM per device.

v0:
```python
import math

import jax
import jax.numpy as jnp
from jax import lax
from jax.sharding import PartitionSpec as P

HEAD_DIM = 64
POOL_WIDTH = 1024
POOL_GROUPS = 4


epsilon = 1e-06
masked_fill = -1e30


def from_behind(value, axis, steps):
    count = lax.axis_size(axis)
    leading, last = (max(0, -steps), min(count, count - steps))
    return lax.ppermute(value, axis, [(source, source + steps) for source in range(leading, last)])


def rms_scale(values, gain):
    return values * lax.rsqrt(jnp.mean(values * values, axis=-1, keepdims=True) + epsilon) * gain


def block_partials(query_rows, query_pos, query_gate, key_rows, value_rows, key_pos, key_gate):
    logits = jnp.einsum("qhd,gkhd->qhgk", query_rows, key_rows, preferred_element_type=jnp.float32)
    logits = logits + query_gate[:, :, None, None] - jnp.transpose(key_gate, (2, 0, 1))[None]
    allowed = key_pos[None, None, :, :] <= query_pos[:, None, None, None]
    logits = jnp.where(allowed, logits, masked_fill)
    block_max = jnp.max(logits, axis=-1)
    weights = jnp.where(allowed, jnp.exp(logits - block_max[..., None]), 0.0)
    totals = jnp.sum(weights, axis=-1)
    numerator = jnp.einsum(
        "qhgk,gkhd->qhgd",
        weights.astype(jnp.bfloat16),
        value_rows,
        preferred_element_type=jnp.float32,
    )
    return (block_max, totals, numerator)


def merge_state(state, partials):
    run_max, run_den, run_acc = state
    block_max, totals, numerator = partials
    new_max = jnp.maximum(run_max, jnp.max(block_max, axis=-1))
    old_scale = jnp.exp(run_max - new_max)
    block_scale = jnp.exp(block_max - new_max[..., None])
    new_den = run_den * old_scale + jnp.sum(block_scale * totals, axis=-1)
    new_acc = run_acc * old_scale[..., None] + jnp.sum(block_scale[..., None] * numerator, axis=2)
    return (new_max, new_den, new_acc)


def empty_state(rows, heads_here):
    return (
        jnp.full((rows, heads_here), masked_fill, jnp.float32),
        jnp.zeros((rows, heads_here), jnp.float32),
        jnp.zeros((rows, heads_here, HEAD_DIM), jnp.float32),
    )


def per_device(
    tokens,
    norm_gain,
    query_weight,
    key_weight,
    value_weight,
    pool_weight,
    query_gain,
    key_gain,
    cum_gate,
    out_pool_weight,
    out_attn_weight,
):
    full_rows = lax.all_gather(tokens, "tp", axis=1, tiled=True)
    normed = rms_scale(full_rows.astype(jnp.float32), norm_gain).astype(jnp.bfloat16)
    length = full_rows.shape[0]
    heads_here = cum_gate.shape[1]
    offset = lax.axis_index("sp") * length

    def project(weight):
        return lax.dot_general(
            normed, weight, (((1,), (1,)), ((), ())), preferred_element_type=jnp.float32
        )

    query_heads = (
        rms_scale(project(query_weight).reshape(length, heads_here, HEAD_DIM), query_gain)
        * HEAD_DIM ** (-0.5)
    ).astype(jnp.bfloat16)
    key_heads = rms_scale(
        project(key_weight).reshape(length, heads_here, HEAD_DIM), key_gain
    ).astype(jnp.bfloat16)
    value_heads = project(value_weight).astype(jnp.bfloat16).reshape(length, heads_here, HEAD_DIM)
    pool_input = project(pool_weight).astype(jnp.bfloat16)
    reach = 2**POOL_GROUPS
    rim_rows = from_behind(pool_input[length - reach :], "sp", 1)
    extended = jnp.concatenate([rim_rows, pool_input], axis=0).astype(jnp.float32)
    prefix = jnp.cumsum(extended, axis=0)
    width_here = pool_input.shape[1]
    channel_ids = lax.axis_index("tp") * width_here + jnp.arange(width_here, dtype=jnp.int32)
    group_ids = channel_ids // (POOL_WIDTH // POOL_GROUPS)
    counts = (offset + jnp.arange(1, length + 1, dtype=jnp.int32)).astype(jnp.float32)[:, None]
    current = prefix[reach:]
    pooled_mean = jnp.zeros((length, width_here), jnp.float32)
    for group_index in range(POOL_GROUPS):
        window = 2 ** (group_index + 1)
        lagged = prefix[reach - window : reach - window + length]
        average = (current - lagged) / jnp.minimum(counts, float(window))
        pooled_mean = jnp.where(group_ids[None, :] == group_index, average, pooled_mean)
    pooled = (pooled_mean - extended[reach:]).astype(jnp.bfloat16)
    gate_all = lax.all_gather(cum_gate, "sp", axis=0, tiled=True)
    query_pos = offset + jnp.arange(length, dtype=jnp.int32)
    key_flat = key_heads.reshape(length, heads_here * HEAD_DIM)
    value_flat = value_heads.reshape(length, heads_here * HEAD_DIM)

    def absorb(carried, inputs):
        key_rows, value_rows, key_gate, key_pos = inputs
        partials = block_partials(
            query_heads, query_pos, cum_gate, key_rows, value_rows, key_pos, key_gate
        )
        return (merge_state(carried, partials), None)

    key_piece = lax.all_gather(key_flat, "sp", axis=0, tiled=True)
    value_piece = lax.all_gather(value_flat, "sp", axis=0, tiled=True)
    shards = key_piece.shape[0] // length
    grouping = math.gcd(shards, 8)
    turns = shards // grouping
    key_groups = key_piece.reshape(turns, grouping, length, heads_here, HEAD_DIM)
    value_groups = value_piece.reshape(turns, grouping, length, heads_here, HEAD_DIM)
    gate_groups = gate_all.reshape(turns, grouping, length, heads_here)
    pos_groups = jnp.arange(shards * length, dtype=jnp.int32).reshape(turns, grouping, length)
    result, _ = lax.scan(
        absorb, empty_state(length, heads_here), (key_groups, value_groups, gate_groups, pos_groups)
    )
    final_max, final_den, final_acc = result
    attended = (
        (final_acc / final_den[..., None])
        .reshape(length, heads_here * HEAD_DIM)
        .astype(jnp.bfloat16)
    )
    pool_full, attn_full = (
        lax.all_gather(pooled, "tp", axis=1, tiled=True),
        lax.all_gather(attended, "tp", axis=1, tiled=True),
    )
    output = jnp.dot(pool_full, out_pool_weight, preferred_element_type=jnp.float32) + jnp.dot(
        attn_full, out_attn_weight, preferred_element_type=jnp.float32
    )
    return output.astype(jnp.bfloat16)


def solution(mesh):
    return jax.shard_map(
        per_device,
        mesh=mesh,
        in_specs=(
            P("sp", "tp"),
            P(),
            P("tp", None),
            P("tp", None),
            P("tp", None),
            P("tp", None),
            P(),
            P(),
            P("sp", "tp"),
            P(None, "tp"),
            P(None, "tp"),
        ),
        out_specs=P("sp", "tp"),
        check_vma=False,
    )
```

profile of v0, /device:TPU:0, one launch (start us, length us, event | category | flops | bytes accessed | tf_op | source)
XLA Modules:
  0.0 260.2 jit_solution(4839599759511507353)
XLA Ops:
  8.0 12.6 %all-gather.4.cloned.1.call-done = bf16[256,2048]{1,0:T(8,128)(2,1)} async-done(((bf16[256,1024]{1,0:T(8,128)(2,1)}), bf16[256,2048]{1,0:T(8,128)(2,1)}) %all-gather.4.cloned.1.call-update) | async-done | bytes 1048592 | tf_op jit(solution)/shard_map/all_gather | solution.py:76
  20.7 1.5 fusion.24
  22.2 2.8 %fusion.50 = (f32[256,512]{1,0:T(8,128)S(1)}, f32[256,512]{1,0:T(8,128)}) fusion(bf16[512,2048]{1,0:T(8,128)(2,1)S(1)} %copy-done, bf16[256,2048]{1,0:T(8,128)(2,1)} %all-gather.4.cloned.1.call-done, f32[2048]{0:T(1024)} %param.14, f32[256]{0:T(256)S(1)} %add_rsqrt_fusion.2), kind=kOutput, calls=%fused_computation.93 | convolution fusion | flops 539099136 | bytes 4203520 | tf_op jit(solution)/shard_map/dot_general | solution.py:83
  26.9 3.0 %convolution_convert_fusion = bf16[256,512]{1,0:T(8,128)(2,1)} fusion(bf16[512,2048]{1,0:T(8,128)(2,1)} %param.17, bf16[256,2048]{1,0:T(8,128)(2,1)S(1)} %copy-done.4, f32[2048]{0:T(1024)S(1)} %copy-done.9, f32[256]{0:T(256)S(1)} %add_rsqrt_fusion.2), kind=kOutput, calls=%fused_computation.41 | convolution fusion | flops 539099136 | bytes 3417088 | tf_op jit(solution)/shard_map/dot_general | solution.py:83
  30.0 42.8 %all_gather.21 = f32[4096,8]{0,1:T(8,128)S(1)} all-gather(f32[256,8]{0,1:T(8,128)S(1)} %copy-done.6), channel_id=1, replica_groups=mesh['sp'=16,'tp'=2] {'sp'}, dimensions={0}, use_global_device_ids=true | all-gather | bytes 139264 | tf_op jit(solution)/shard_map/all_gather | solution.py:112
  72.9 2.5 convolution_convert_fusion.1
  75.4 1.3 collective-permute-start
  80.2 2.5 all_gather.19
  83.4 20.9 %all-gather.6.cloned.1.call-done = bf16[4096,512]{1,0:T(8,128)(2,1)} async-done(((bf16[256,512]{1,0:T(8,128)(2,1)}), bf16[4096,512]{1,0:T(8,128)(2,1)}) %all-gather.6.cloned.1.call-update) | async-done | bytes 4194320 | tf_op jit(solution)/shard_map/all_gather | solution.py:124
  104.3 11.2 %reshape.154 = bf16[2,8,256,8,64]{4,3,2,1,0:T(8,128)(2,1)} reshape(bf16[4096,512]{1,0:T(8,128)(2,1)} %all-gather.6.cloned.1.call-done) | data formatting | bytes 8388608 | tf_op jit(solution)/shard_map/reshape | solution.py:129
  115.5 9.8 %copy.42 = bf16[2,8,256,8,64]{2,4,1,3,0:T(8,128)(2,1)} copy(bf16[2,8,256,8,64]{4,3,2,1,0:T(8,128)(2,1)} %reshape.154) | data formatting | bytes 8388608
  125.3 56.0 %all-gather.8.cloned.1.call-done = bf16[4096,512]{1,0:T(8,128)(2,1)} async-done(((bf16[256,512]{1,0:T(8,128)(2,1)}), bf16[4096,512]{1,0:T(8,128)(2,1)}) %all-gather.8.cloned.1.call-update) | async-done | bytes 4194320 | tf_op jit(solution)/shard_map/all_gather | solution.py:125
  181.3 11.2 %reshape.155 = bf16[2,8,256,8,64]{4,3,2,1,0:T(8,128)(2,1)} reshape(bf16[4096,512]{1,0:T(8,128)(2,1)} %all-gather.8.cloned.1.call-done) | data formatting | bytes 8388608 | tf_op jit(solution)/shard_map/reshape | solution.py:130
  192.5 9.8 %copy.44 = bf16[2,8,256,8,64]{2,4,1,3,0:T(8,128)(2,1)} copy(bf16[2,8,256,8,64]{4,3,2,1,0:T(8,128)(2,1)} %reshape.155) | data formatting | bytes 8388608
  202.2 46.0 %while.15 = (s32[]{:T(128)}, f32[256,8]{0,1:T(8,128)S(1)}, f32[256,8]{0,1:T(8,128)S(1)}, f32[256,8,64]{0,2,1:T(8,128)S(1)}, s32[2,8,256]{2,1,0:T(8,128)S(1)}, /*...) while((s32[]{:T(128)}, f32[256,8]{0,1:T(8,128)S(1)}, ...), condition=%wide.region_11.12_spmd.clone, body=%wide.region_5.11_spmd.clone.sunk | while | flops 1122789632 | bytes 127101120 | solution.py:133
  202.8 6.9 %fusion.69 = (f32[256,8,8]{0,2,1:T(8,128)S(1)}, f32[256,8,8,256]{0,3,2,1:T(8,128)S(1)}) fusion(f32[8,8,256]{2,1,0:T(8,128)S(1)} %bitcast.72, f32[256,8]{0,1:T(8,128)S(1)} %get-tuple-element.297, bf16[256,8,64]{0,2,1:T(8,128)(2,1)S(1)} %get-tuple-element.296, bf16[2,8,256,8,64]{2,4,1,3,0:T(8,128)(2,1)} %get-tuple-element.295, s32[]{:T(128)S(6)} %copy.63, ...), kind=kOutput, calls=%fused_computation.92.clone.1 | convolution fusion | flops 553631744 | bytes 19800068 | tf_op jit(solution)/shard_map/while/body/eval_jaxpr/qhd,gkhd->qhgk/dot_general | solution.py:28
  209.7 4.8 %fusion.70 = (f32[256,8,8]{0,2,1:T(8,128)S(1)}, f32[256,8]{0,1:T(8,128)S(1)}) fusion(f32[256,8,8,256]{0,3,2,1:T(8,128)S(1)} %get-tuple-element.256, f32[256,8,8]{0,2,1:T(8,128)S(1)} %get-tuple-element.257, pred[256,8,256]{0,2,1:T(8,128)(4,1)S(1)} %broadcast_compare_fusion.6), kind=kLoop, calls=%fused_computation.6.clone.1 | loop fusion | flops 16758784 | bytes 17440768 | tf_op jit(solution)/shard_map/while/body/eval_jaxpr/reduce_sum | solution.py:34
  214.5 0.9 copy-done.2
  215.5 9.5 %fusion.72 = f32[256,8,64]{0,2,1:T(8,128)S(1)} fusion(f32[256,8,8,256]{0,3,2,1:T(8,128)} %copy-done.2, f32[256,8,8]{0,2,1:T(8,128)S(1)} %get-tuple-element.257, pred[256,8,256]{0,2,1:T(8,128)(4,1)S(1)} %broadcast_compare_fusion.6, bf16[2,8,256,8,64]{2,4,1,3,0:T(8,128)(2,1)} %get-tuple-element.299, s32[]{:T(128)S(6)} %copy.63, ...), kind=kOutput, calls=%fused_computation.12.clone.1 | convolution fusion | flops 551419904 | bytes 20054020 | tf_op jit(solution)/shard_map/while/body/eval_jaxpr/qhgk,gkhd->qhgd/dot_general | solution.py:35
  225.8 6.9 %fusion.69 = (f32[256,8,8]{0,2,1:T(8,128)S(1)}, f32[256,8,8,256]{0,3,2,1:T(8,128)S(1)}) fusion(f32[8,8,256]{2,1,0:T(8,128)S(1)} %bitcast.72, f32[256,8]{0,1:T(8,128)S(1)} %get-tuple-element.297, bf16[256,8,64]{0,2,1:T(8,128)(2,1)S(1)} %get-tuple-element.296, bf16[2,8,256,8,64]{2,4,1,3,0:T(8,128)(2,1)} %get-tuple-element.295, s32[]{:T(128)S(6)} %copy.63, ...), kind=kOutput, calls=%fused_computation.92.clone.1 | convolution fusion | flops 553631744 | bytes 19800068 | tf_op jit(solution)/shard_map/while/body/eval_jaxpr/qhd,gkhd->qhgk/dot_general | solution.py:28
  232.7 4.8 %fusion.70 = (f32[256,8,8]{0,2,1:T(8,128)S(1)}, f32[256,8]{0,1:T(8,128)S(1)}) fusion(f32[256,8,8,256]{0,3,2,1:T(8,128)S(1)} %get-tuple-element.256, f32[256,8,8]{0,2,1:T(8,128)S(1)} %get-tuple-element.257, pred[256,8,256]{0,2,1:T(8,128)(4,1)S(1)} %broadcast_compare_fusion.6), kind=kLoop, calls=%fused_computation.6.clone.1 | loop fusion | flops 16758784 | bytes 17440768 | tf_op jit(solution)/shard_map/while/body/eval_jaxpr/reduce_sum | solution.py:34
  238.5 9.5 %fusion.72 = f32[256,8,64]{0,2,1:T(8,128)S(1)} fusion(f32[256,8,8,256]{0,3,2,1:T(8,128)} %copy-done.2, f32[256,8,8]{0,2,1:T(8,128)S(1)} %get-tuple-element.257, pred[256,8,256]{0,2,1:T(8,128)(4,1)S(1)} %broadcast_compare_fusion.6, bf16[2,8,256,8,64]{2,4,1,3,0:T(8,128)(2,1)} %get-tuple-element.299, s32[]{:T(128)S(6)} %copy.63, ...), kind=kOutput, calls=%fused_computation.12.clone.1 | convolution fusion | flops 551419904 | bytes 20054020 | tf_op jit(solution)/shard_map/while/body/eval_jaxpr/qhgk,gkhd->qhgd/dot_general | solution.py:35
  248.3 2.3 all_gather.23
  250.6 3.1 %fusion.27 = bf16[256,1024]{1,0:T(8,128)(2,1)} fusion(f32[256,1024]{1,0:T(8,128)S(1)} %fusion.51, bf16[256,1024]{0,1:T(8,128)(2,1)S(1)} %all_gather.23, bf16[1024,1024]{1,0:T(8,128)(2,1)} %param.23), kind=kOutput, calls=%fused_computation.40 | convolution fusion | flops 537395200 | bytes 4194304 | tf_op jit(solution)/shard_map/dot_general | solution.py:146
  (79 shorter events, 10.0 us)
Async XLA Ops:
  6.5 15.6 %copy-start = (bf16[512,2048]{1,0:T(8,128)(2,1)S(1)}, bf16[512,2048]{1,0:T(8,128)(2,1)}, u32[]{:S(2)}) copy-start(bf16[512,2048]{1,0:T(8,128)(2,1)} %param.16) | copy-start | bytes 6291460
  6.5 14.1 %all-gather.4.cloned.1.call-start = ((), (), s32[]{:S(2)}) async-start(), calls=%async_computation | async-start | bytes 1572864 | tf_op jit(solution)/shard_map/all_gather | solution.py:76
  7.3 97.0 %all-gather.6.cloned.1.call-start = ((), (), s32[]{:S(2)}) async-start(), calls=%async_computation.1 | async-start | bytes 4456448 | tf_op jit(solution)/shard_map/all_gather | solution.py:124
  25.0 1.0 copy-start.5
  25.2 1.7 copy-start.4
  25.2 1.7 copy-start.9
  26.8 3.2 %copy-start.6 = (f32[256,8]{0,1:T(8,128)S(1)}, f32[256,8]{0,1:T(8,128)}, u32[]{:S(2)}) copy-start(f32[256,8]{0,1:T(8,128)} %param.21) | copy-start | bytes 24580
  26.9 154.4 %all-gather.8.cloned.1.call-start = ((), (), s32[]{:S(2)}) async-start(), calls=%async_computation.2 | async-start | bytes 4456448 | tf_op jit(solution)/shard_map/all_gather | solution.py:125
  72.9 3.8 %copy-start.8 = (bf16[512,2048]{1,0:T(8,128)(2,1)S(1)}, bf16[512,2048]{1,0:T(8,128)(2,1)}, u32[]{:S(2)}) copy-start(bf16[512,2048]{1,0:T(8,128)(2,1)} %param.15) | copy-start | bytes 6291460
  75.4 2.2 copy-start.7
  75.4 3.0 %collective-permute-start = (bf16[16,512]{1,0:T(8,128)(2,1)S(1)}, bf16[16,512]{1,0:T(8,128)(2,1)S(1)}, u32[]{:S(2)}, u32[]{:S(2)}) collective-permute-start(bf16[16,512]{1,0:T(8,128)(2,1)S(1)} %slice.42), channel_id=1, source_target_pairs={{0,2},{2,4},{4,6},{6,8},{8,10},{10,12},{12,14},{14,16},{16,18},{18... | collective-permute-start | bytes 49160 | tf_op jit(solution)/shard_map/ppermute | solution.py:20
  79.7 3.0 %copy-start.3 = (bf16[1024,1024]{1,0:T(8,128)(2,1)S(1)}, bf16[1024,1024]{1,0:T(8,128)(2,1)}, u32[]{:S(2)}) copy-start(bf16[1024,1024]{1,0:T(8,128)(2,1)} %param.22) | copy-start | bytes 6291460
  209.7 5.7 %copy-start.2 = (f32[256,8,8,256]{0,3,2,1:T(8,128)}, f32[256,8,8,256]{0,3,2,1:T(8,128)S(1)}, u32[]{:S(2)}) copy-start(f32[256,8,8,256]{0,3,2,1:T(8,128)S(1)} %get-tuple-element.256) | copy-start | bytes 50331652 | tf_op jit(solution)/shard_map/while
  232.7 5.7 %copy-start.2 = (f32[256,8,8,256]{0,3,2,1:T(8,128)}, f32[256,8,8,256]{0,3,2,1:T(8,128)S(1)}, u32[]{:S(2)}) copy-start(f32[256,8,8,256]{0,3,2,1:T(8,128)S(1)} %get-tuple-element.256) | copy-start | bytes 50331652 | tf_op jit(solution)/shard_map/while
  248.2 5.4 %copy-start.1 = (bf16[512,2048]{1,0:T(8,128)(2,1)S(1)}, bf16[512,2048]{1,0:T(8,128)(2,1)}, u32[]{:S(2)}) copy-start(bf16[512,2048]{1,0:T(8,128)(2,1)} %param.16) | copy-start | bytes 6291460
Sparse Core Ops, SparseCore 0:
  8.9 11.7 all-gather.3
  27.0 77.2 all-gather.5
  107.1 74.1 all-gather.7
where the time goes:
time: 262 us; the launch traced here: 260 us
  waiting for transfers between devices  90.9 us (35%)
  blocking collectives  47.6 us (18%)
  local copies, waits for them, and re-layouts  45.9 us (18%)
  matrix products  45.8 us (17%)
  other arithmetic  15 us (6%)
  between operations  13.4 us (5%)
    all_gather x1, waiting for transfers between devices, per_device(): value_piece = lax.all_gather(value_flat, 'sp', axis=0, tiled=True)  56 us
    all_gather x1, blocking collectives, per_device(): gate_all = lax.all_gather(cum_gate, 'sp', axis=0, tiled=True)  42.8 us
    all_gather x1, waiting for transfers between devices, per_device(): key_piece = lax.all_gather(key_flat, 'sp', axis=0, tiled=True)  20.9 us
    unnamed x20, local copies, waits for them, and re-layouts  20.1 us
    dot_general x2, matrix products, block_partials(): jnp.einsum('qhgk,gkhd->qhgd', weights.astype(jnp.bfloat16), value_rows, p...  19 us
    dot_general x2, matrix products, block_partials(): jnp.einsum('qhd,gkhd->qhgk', query_rows, key_rows, preferred_element_type...  13.8 us
    all_gather x1, waiting for transfers between devices, per_device(): full_rows = lax.all_gather(tokens, 'tp', axis=1, tiled=True)  12.6 us
    reshape x1, local copies, waits for them, and re-layouts, per_device(): key_piece.reshape(turns, grouping, length, heads_here, HEAD_DIM)  11.2 us
  transfers between devices with their start and end apart: 4, of which 4 were waited for; matrix products, arithmetic and copies ran while one was open for 12% of the time, Pallas kernels for 0%

commit v1 on v0

v1 whole, which is shorter than its diff:
```python
import functools

import jax
import jax.numpy as jnp
from jax import lax
from jax.experimental import pallas as pl
from jax.experimental.pallas import tpu as pltpu
from jax.sharding import PartitionSpec as P

HEAD_DIM = 64
POOL_WIDTH = 1024
POOL_GROUPS = 4
PAD = 16
KEY_ROWS = HEAD_DIM + PAD
REACH = 2**POOL_GROUPS

epsilon = 1e-06
masked_fill = -1e30
MESH = pl.DeviceIdType.MESH
NT = (((1,), (1,)), ((), ()))
TN = (((0,), (0,)), ((), ()))
NN = (((1,), (0,)), ((), ()))


def dot(a, b, dims):
    return lax.dot_general(a, b, dims, preferred_element_type=jnp.float32)


def split3(x):
    hi = x.astype(jnp.bfloat16).astype(jnp.float32)
    mid = (x - hi).astype(jnp.bfloat16).astype(jnp.float32)
    low = (x - hi - mid).astype(jnp.bfloat16).astype(jnp.float32)
    return hi, mid, low


def kernel(
    n, T, R, Hh,
    tok, ngain, wq_h, wk_h, wv_h, wp_h, qg, kg, gT, wop_h, woa_h,
    out,
    tokf, nrm, wq, wk, wv, wp, wop, woa, kvs, qs, kvr, qr,
    ext, rim, poolf, att_s, attf, total,
    wsem, tok_ss, tok_rs, kv_ss, kv_rs, q_ss, q_rs, rim_ss, rim_rs,
    pf_ss, pf_rs, at_ss, at_rs, af_ss, af_rs,
):
    me = lax.axis_index("sp")
    t = lax.axis_index("tp")
    L = tok.shape[0]
    F = Hh * HEAD_DIM
    my_head = me // R
    my_r = lax.rem(me, R)
    phase = lax.rem(me, 2 * R)
    out_r = jnp.where(phase < R, phase, 2 * R - 1 - phase)
    out_slot = 2 * (me // (2 * R)) + jnp.where(phase < R, 0, 1)

    def block_of(s):
        return (s // 2) * 2 * R + jnp.where(lax.rem(s, 2) == 0, my_r, 2 * R - 1 - my_r)

    weights = [(wk_h, wk), (wv_h, wv), (wq_h, wq), (wp_h, wp), (wop_h, wop), (woa_h, woa)]
    loads = [pltpu.make_async_copy(a, b, wsem.at[i]) for i, (a, b) in enumerate(weights)]
    for load in loads:
        load.start()

    barrier = pltpu.get_barrier_semaphore()

    @pl.loop(1, n)
    def _(o):
        pl.semaphore_signal(
            barrier, inc=1, device_id=(lax.rem(me + o, n), t), device_id_type=MESH
        )

    for o in range(1, T):
        pl.semaphore_signal(
            barrier, inc=1, device_id=(me, lax.rem(t + o, T)), device_id_type=MESH
        )
    pl.semaphore_wait(barrier, n - 1 + T - 1)

    def sibling(src, dst, ss, rs):
        return [
            pltpu.make_async_remote_copy(
                src_ref=src, dst_ref=dst, send_sem=ss.at[o - 1], recv_sem=rs.at[o - 1],
                device_id=(me, lax.rem(t + o, T)), device_id_type=MESH,
            )
            for o in range(1, T)
        ]

    tok_copies = sibling(tok, tokf.at[t], tok_ss, tok_rs)
    for c in tok_copies:
        c.start()
    tokf[t] = tok[...]
    for c in tok_copies:
        c.wait()

    Dt = tok.shape[1]
    square = jnp.zeros((L, 1), jnp.float32)
    for i in range(T):
        x = tokf[i].astype(jnp.float32)
        square += jnp.sum(x * x, axis=-1, keepdims=True)
    scale = lax.rsqrt(square / (T * Dt) + epsilon)
    for i in range(T):
        cols = slice(i * Dt, (i + 1) * Dt)
        x = tokf[i].astype(jnp.float32)
        nrm[:, cols] = (x * scale * ngain[:, cols]).astype(jnp.bfloat16)

    def head_norm(y, gain):
        y = y.reshape(Hh, HEAD_DIM, L)
        ms = jnp.mean(y * y, axis=1, keepdims=True)
        return y * lax.rsqrt(ms + epsilon) * gain[...][None]

    ghi, gmid, glow = split3(gT[...])
    row = lax.broadcasted_iota(jnp.int32, (PAD, L), 0)

    def gate_rows(h, sign, first):
        pad = jnp.where((row >= 3 - first) & (row < 6 - first), 1.0, 0.0)
        for k, part in enumerate((ghi, gmid, glow)):
            pad = jnp.where(row == k + first, sign * part[h : h + 1], pad)
        return pad.astype(jnp.bfloat16)

    loads[0].wait()
    kvs[:, :HEAD_DIM] = head_norm(dot(wk[...], nrm[...], NT), kg).astype(jnp.bfloat16)
    for h in range(Hh):
        kvs[h, HEAD_DIM:KEY_ROWS] = gate_rows(h, -1.0, 0)
    loads[1].wait()
    kvs[:, KEY_ROWS:] = (
        dot(wv[...], nrm[...], NT).astype(jnp.bfloat16).reshape(Hh, HEAD_DIM, L)
    )

    def kv_copy(o):
        to = lax.rem(me + o, n)
        return pltpu.make_async_remote_copy(
            src_ref=kvs.at[to // R], dst_ref=kvr.at[me],
            send_sem=kv_ss.at[o - 1], recv_sem=kv_rs.at[o - 1],
            device_id=(to, t), device_id_type=MESH,
        )

    def kv_arrival(o):
        return pltpu.make_async_remote_copy(
            src_ref=kvs.at[0], dst_ref=kvr.at[lax.rem(me - o + n, n)],
            send_sem=kv_ss.at[o - 1], recv_sem=kv_rs.at[o - 1],
            device_id=(lax.rem(me + o, n), t), device_id_type=MESH,
        )

    @pl.loop(1, n)
    def _(o):
        kv_copy(o).start()

    kvr[me] = kvs[my_head]

    loads[2].wait()
    q = head_norm(dot(wq[...], nrm[...], NT), qg) * HEAD_DIM ** (-0.5)
    qs[:, :HEAD_DIM] = q.astype(jnp.bfloat16)
    for h in range(Hh):
        qs[h, HEAD_DIM:KEY_ROWS] = gate_rows(h, 1.0, 3)

    def q_copy(h):
        return pltpu.make_async_remote_copy(
            src_ref=qs.at[h], dst_ref=qr.at[out_slot],
            send_sem=q_ss.at[h], recv_sem=q_rs.at[out_slot],
            device_id=(h * R + out_r, t), device_id_type=MESH,
        )

    def q_arrival(s):
        return pltpu.make_async_remote_copy(
            src_ref=qs.at[0], dst_ref=qr.at[s],
            send_sem=q_ss.at[0], recv_sem=q_rs.at[s],
            device_id=(block_of(s), t), device_id_type=MESH,
        )

    @pl.loop(0, Hh)
    def _(h):
        @pl.when(h * R + out_r != me)
        def _():
            q_copy(h).start()

        @pl.when(h * R + out_r == me)
        def _():
            qr[out_slot] = qs[h]

    loads[3].wait()
    pool_input = dot(nrm[...], wp[...], NT).astype(jnp.bfloat16)
    ext[...] = pool_input[L - REACH :]
    rim_copy = pltpu.make_async_remote_copy(
        src_ref=ext, dst_ref=rim, send_sem=rim_ss, recv_sem=rim_rs,
        device_id=(lax.rem(me + 1, n), t), device_id_type=MESH,
    )

    rim_copy.start()
    rim_copy.wait()
    before = jnp.where(me == 0, 0.0, rim[...].astype(jnp.float32))
    current = pool_input.astype(jnp.float32)
    running = jnp.concatenate([before, current], axis=0)
    width_here = current.shape[1]
    channel = t * width_here + lax.broadcasted_iota(jnp.int32, (1, width_here), 1)
    group = channel // (POOL_WIDTH // POOL_GROUPS)
    counts = (me * L + 1 + lax.broadcasted_iota(jnp.int32, (L, 1), 0)).astype(jnp.float32)
    pooled = jnp.zeros_like(current)
    for g in range(POOL_GROUPS):
        lag = 2**g
        running = running + jnp.concatenate(
            [jnp.zeros((lag, width_here), jnp.float32), running[:-lag]], axis=0
        )
        average = running[REACH:] / jnp.minimum(counts, float(2 * lag))
        pooled = jnp.where(group == g, average, pooled)
    poolf[t] = (pooled - current).astype(jnp.bfloat16)
    pool_copies = sibling(poolf.at[t], poolf.at[t], pf_ss, pf_rs)
    for c in pool_copies:
        c.start()

    @pl.loop(1, n)
    def _(o):
        kv_arrival(o).wait_recv()

    def scores(q_block, j):
        return dot(kvr[j, :KEY_ROWS], q_block, TN)

    def absorb(state, s, values):
        top, den, acc = state
        new_top = jnp.maximum(top, jnp.max(s, axis=0, keepdims=True))
        old = jnp.exp(top - new_top)
        w = jnp.exp(s - new_top)
        den = den * old + jnp.sum(w, axis=0, keepdims=True)
        acc = acc * old + dot(values, w.astype(jnp.bfloat16), NN)
        return new_top, den, acc

    allowed = lax.broadcasted_iota(jnp.int32, (L, L), 0) <= lax.broadcasted_iota(
        jnp.int32, (L, L), 1
    )

    def at_copy(s):
        return pltpu.make_async_remote_copy(
            src_ref=att_s.at[s], dst_ref=attf.at[t, my_head],
            send_sem=at_ss.at[s], recv_sem=at_rs.at[my_head],
            device_id=(block_of(s), t), device_id_type=MESH,
        )

    def at_arrival(h):
        return pltpu.make_async_remote_copy(
            src_ref=att_s.at[0], dst_ref=attf.at[t, h],
            send_sem=at_ss.at[0], recv_sem=at_rs.at[h],
            device_id=(h * R + out_r, t), device_id_type=MESH,
        )

    @pl.loop(0, Hh)
    def _(s):
        b = block_of(s)

        @pl.when(b != me)
        def _():
            q_arrival(s).wait_recv()

        q_block = qr[s]
        first = jnp.where(allowed, scores(q_block, b), masked_fill)
        state = (
            jnp.full((1, L), masked_fill, jnp.float32),
            jnp.zeros((1, L), jnp.float32),
            jnp.zeros((HEAD_DIM, L), jnp.float32),
        )
        state = absorb(state, first, kvr[b, KEY_ROWS:])

        def single(j, state):
            return absorb(state, scores(q_block, j), kvr[j, KEY_ROWS:])

        def pair(p, state):
            j = 2 * p
            both = jnp.concatenate([scores(q_block, j), scores(q_block, j + 1)], axis=0)
            values = jnp.concatenate([kvr[j, KEY_ROWS:], kvr[j + 1, KEY_ROWS:]], axis=1)
            return absorb(state, both, values)

        state = lax.fori_loop(0, b // 2, pair, state)
        state = lax.fori_loop(2 * (b // 2), b, single, state)
        att_s[s] = (state[2] / state[1]).astype(jnp.bfloat16)

        @pl.when(b != me)
        def _():
            at_copy(s).start()

        @pl.when(b == me)
        def _():
            attf[t, my_head] = att_s[s]

    for c in pool_copies:
        c.wait()
    loads[4].wait()
    for i in range(T):
        part = dot(poolf[i], wop[i * width_here : (i + 1) * width_here], NN)
        if i == 0:
            total[...] = part
        else:
            total[...] += part

    @pl.loop(0, Hh)
    def _(h):
        @pl.when(h * R + out_r != me)
        def _():
            at_arrival(h).wait_recv()

    att_copies = sibling(attf.at[t], attf.at[t], af_ss, af_rs)
    for c in att_copies:
        c.start()
    loads[5].wait()

    def attn_part(i):
        rows = pl.ds(pl.multiple_of(i * F, F), F)
        return dot(attf[i].reshape(F, L), woa[rows], TN)

    result = total[...] + attn_part(t)
    for o in range(1, T):
        att_copies[o - 1].wait()
        result = result + attn_part(lax.rem(t - o + T, T))
    out[...] = result.astype(jnp.bfloat16)

    @pl.loop(1, n)
    def _(o):
        kv_copy(o).wait_send()

    @pl.loop(0, Hh)
    def _(h):
        @pl.when(h * R + out_r != me)
        def _():
            q_copy(h).wait_send()

        @pl.when(block_of(h) != me)
        def _():
            at_copy(h).wait_send()


def solution(mesh):
    n, T = mesh.shape["sp"], mesh.shape["tp"]

    def per_device(
        tokens, norm_gain, query_weight, key_weight, value_weight, pool_weight,
        query_gain, key_gain, cum_gate, out_pool_weight, out_attn_weight,
    ):
        L, Dt = tokens.shape
        Hh = cum_gate.shape[1]
        R = n // Hh
        F = Hh * HEAD_DIM
        Fp = pool_weight.shape[0]
        bf, f32 = jnp.bfloat16, jnp.float32
        vmem = pl.BlockSpec(memory_space=pltpu.VMEM)
        hbm = pl.BlockSpec(memory_space=pl.ANY)
        dma = pltpu.SemaphoreType.DMA
        S = max(T - 1, 1)
        return pl.pallas_call(
            functools.partial(kernel, n, T, R, Hh),
            out_shape=jax.ShapeDtypeStruct((L, Dt), bf),
            in_specs=[vmem, vmem, hbm, hbm, hbm, hbm, vmem, vmem, vmem, hbm, hbm],
            out_specs=vmem,
            scratch_shapes=[
                pltpu.VMEM((T, L, Dt), bf),
                pltpu.VMEM((L, T * Dt), bf),
                pltpu.VMEM(query_weight.shape, bf),
                pltpu.VMEM(key_weight.shape, bf),
                pltpu.VMEM(value_weight.shape, bf),
                pltpu.VMEM(pool_weight.shape, bf),
                pltpu.VMEM(out_pool_weight.shape, bf),
                pltpu.VMEM(out_attn_weight.shape, bf),
                pltpu.VMEM((Hh, KEY_ROWS + HEAD_DIM, L), bf),
                pltpu.VMEM((Hh, KEY_ROWS, L), bf),
                pltpu.VMEM((n, KEY_ROWS + HEAD_DIM, L), bf),
                pltpu.VMEM((Hh, KEY_ROWS, L), bf),
                pltpu.VMEM((REACH, Fp), bf),
                pltpu.VMEM((REACH, Fp), bf),
                pltpu.VMEM((T, L, Fp), bf),
                pltpu.VMEM((Hh, HEAD_DIM, L), bf),
                pltpu.VMEM((T, Hh, HEAD_DIM, L), bf),
                pltpu.VMEM((L, Dt), f32),
                dma((6,)),
                dma((S,)), dma((S,)),
                dma((n - 1,)), dma((n - 1,)),
                dma((Hh,)), dma((Hh,)),
                dma, dma,
                dma((S,)), dma((S,)),
                dma((Hh,)), dma((Hh,)),
                dma((S,)), dma((S,)),
            ],
            compiler_params=pltpu.CompilerParams(
                collective_id=0, has_side_effects=True, vmem_limit_bytes=56 * 2**20
            ),
        )(
            tokens, norm_gain.reshape(1, -1), query_weight, key_weight, value_weight,
            pool_weight, query_gain.reshape(-1, 1), key_gain.reshape(-1, 1), cum_gate.T,
            out_pool_weight, out_attn_weight,
        )

    return jax.shard_map(
        per_device,
        mesh=mesh,
        in_specs=(
            P("sp", "tp"), P(), P("tp", None), P("tp", None), P("tp", None), P("tp", None),
            P(), P(), P("sp", "tp"), P(None, "tp"), P(None, "tp"),
        ),
        out_specs=P("sp", "tp"),
        check_vma=False,
    )
```

time: 262 us -> 75.4 us (0.29)
  the two profiles are of different devices: /device:TPU:0 before, /device:TPU:31 now
where the time goes in v1:
time: 75.4 us; the launch traced here: 75.2 us
  Pallas kernels  70.6 us (94%)
  local copies, waits for them, and re-layouts  4.57 us (6%)
    pallas_call x1, Pallas kernels, per_device(): pl.pallas_call(functools.partial(kernel, n, T, R, Hh), out_shape=jax.Shap...  70.6 us
    unnamed x1, local copies, waits for them, and re-layouts  1.87 us

profile of v1, /device:TPU:31, one launch (start us, length us, event | category | flops | bytes accessed | tf_op | source)
XLA Modules:
  0.0 75.2 jit_solution(9838077963298946454)
XLA Ops:
  0.0 1.4 %copy.12.qg = f32[64,1]{1,0:T(8,128)} copy(f32[64,1]{0,1:T(1,128)} %bitcast.6) | data formatting | bytes 512 | tf_op jit(solution)/shard_map/reshape | solution.py:381
  1.4 1.3 %copy.13.kg = f32[64,1]{1,0:T(8,128)} copy(f32[64,1]{0,1:T(1,128)} %bitcast.7) | data formatting | bytes 512 | tf_op jit(solution)/shard_map/reshape | solution.py:381
  2.7 70.6 %shard_map.109 = bf16[256,1024]{1,0:T(8,128)(2,1)} custom-call(bf16[256,1024]{1,0:T(8,128)(2,1)} %tok.1, f32[1,2048]{1,0:T(1,128)} %bitcast.4, bf16[512,2048]{1,0:T(8,128)(2,1)} %wq_h.1, bf16[512,2048]{1,0:T(8,128)(2,1)} %wk_h.1, bf16[512,2048]{1,0:T(8,128)(2,1)} %wv_h.1, bf16[512,2048]{1,0:T(8,128)(2,1)} %wp_h.1, f32[64,1]{1,0:T(8,128)} %copy.12.qg, ...), custom_call_target="tpu_custom_call" | custom-call | tf_op jit(solution)/shard_map/pallas_call | solution.py:343
  73.3 1.9 %copy.15 = bf16[256,1024]{1,0:T(8,128)(2,1)} copy(bf16[256,1024]{1,0:T(8,128)(2,1)} %shard_map.109) | data formatting | bytes 1048576

commit v2 on v1

--- a/solution.py
+++ b/solution.py
@@ -38,16 +38,21 @@
     tok, ngain, wq_h, wk_h, wv_h, wp_h, qg, kg, gT, wop_h, woa_h,
     out,
     tokf, nrm, wq, wk, wv, wp, wop, woa, kvs, qs, kvr, qr,
-    ext, rim, poolf, att_s, attf, total,
-    wsem, tok_ss, tok_rs, kv_ss, kv_rs, q_ss, q_rs, rim_ss, rim_rs,
+    ext, rim, poolf, att_s, attf, total, keys, top, den, acc,
+    wsem, tok_ss, tok_rs, kv_ss, kv_rs, fw_ss, q_ss, q_rs, rim_ss, rim_rs,
     pf_ss, pf_rs, at_ss, at_rs, af_ss, af_rs,
 ):
     me = lax.axis_index("sp")
     t = lax.axis_index("tp")
     L = tok.shape[0]
     F = Hh * HEAD_DIM
-    my_head = me // R
-    my_r = lax.rem(me, R)
+    C = n // (T * Hh)
+    span = n // T
+    my_tp = me // (C * Hh)
+    my_head = lax.rem(me // C, Hh)
+    my_r = lax.rem(me, C) * T + t
+    relay = lax.rem(me, T)
+    seat = lax.rem(me, span)
     phase = lax.rem(me, 2 * R)
     out_r = jnp.where(phase < R, phase, 2 * R - 1 - phase)
     out_slot = 2 * (me // (2 * R)) + jnp.where(phase < R, 0, 1)
@@ -55,24 +60,21 @@
     def block_of(s):
         return (s // 2) * 2 * R + jnp.where(lax.rem(s, 2) == 0, my_r, 2 * R - 1 - my_r)
 
-    weights = [(wk_h, wk), (wv_h, wv), (wq_h, wq), (wp_h, wp), (wop_h, wop), (woa_h, woa)]
+    weights = [(wq_h, wq), (wk_h, wk), (wv_h, wv), (wp_h, wp), (wop_h, wop), (woa_h, woa)]
     loads = [pltpu.make_async_copy(a, b, wsem.at[i]) for i, (a, b) in enumerate(weights)]
     for load in loads:
         load.start()
 
     barrier = pltpu.get_barrier_semaphore()
 
-    @pl.loop(1, n)
+    @pl.loop(1, n * T)
     def _(o):
+        other = lax.rem(me * T + t + o, n * T)
         pl.semaphore_signal(
-            barrier, inc=1, device_id=(lax.rem(me + o, n), t), device_id_type=MESH
-        )
-
-    for o in range(1, T):
-        pl.semaphore_signal(
-            barrier, inc=1, device_id=(me, lax.rem(t + o, T)), device_id_type=MESH
-        )
-    pl.semaphore_wait(barrier, n - 1 + T - 1)
+            barrier, inc=1, device_id=(other // T, lax.rem(other, T)), device_id_type=MESH
+        )
+
+    pl.semaphore_wait(barrier, n * T - 1)
 
     def sibling(src, dst, ss, rs):
         return [
@@ -104,7 +106,13 @@
     def head_norm(y, gain):
         y = y.reshape(Hh, HEAD_DIM, L)
         ms = jnp.mean(y * y, axis=1, keepdims=True)
-        return y * lax.rsqrt(ms + epsilon) * gain[...][None]
+        square_ids = [
+            lax.broadcasted_iota(jnp.int32, (HEAD_DIM, HEAD_DIM), d) for d in (0, 1)
+        ]
+        column = jnp.sum(
+            jnp.where(square_ids[0] == square_ids[1], gain[...], 0.0), axis=1, keepdims=True
+        )
+        return y * lax.rsqrt(ms + epsilon) * column[None]
 
     ghi, gmid, glow = split3(gT[...])
     row = lax.broadcasted_iota(jnp.int32, (PAD, L), 0)
@@ -116,64 +124,90 @@
         return pad.astype(jnp.bfloat16)
 
     loads[0].wait()
-    kvs[:, :HEAD_DIM] = head_norm(dot(wk[...], nrm[...], NT), kg).astype(jnp.bfloat16)
-    for h in range(Hh):
-        kvs[h, HEAD_DIM:KEY_ROWS] = gate_rows(h, -1.0, 0)
-    loads[1].wait()
-    kvs[:, KEY_ROWS:] = (
-        dot(wv[...], nrm[...], NT).astype(jnp.bfloat16).reshape(Hh, HEAD_DIM, L)
-    )
-
-    def kv_copy(o):
-        to = lax.rem(me + o, n)
-        return pltpu.make_async_remote_copy(
-            src_ref=kvs.at[to // R], dst_ref=kvr.at[me],
-            send_sem=kv_ss.at[o - 1], recv_sem=kv_rs.at[o - 1],
-            device_id=(to, t), device_id_type=MESH,
-        )
-
-    def kv_arrival(o):
-        return pltpu.make_async_remote_copy(
-            src_ref=kvs.at[0], dst_ref=kvr.at[lax.rem(me - o + n, n)],
-            send_sem=kv_ss.at[o - 1], recv_sem=kv_rs.at[o - 1],
-            device_id=(lax.rem(me + o, n), t), device_id_type=MESH,
-        )
-
-    @pl.loop(1, n)
-    def _(o):
-        kv_copy(o).start()
-
-    kvr[me] = kvs[my_head]
-
-    loads[2].wait()
     q = head_norm(dot(wq[...], nrm[...], NT), qg) * HEAD_DIM ** (-0.5)
     qs[:, :HEAD_DIM] = q.astype(jnp.bfloat16)
     for h in range(Hh):
         qs[h, HEAD_DIM:KEY_ROWS] = gate_rows(h, 1.0, 3)
 
+    def is_me(device):
+        return (device[0] == me) & (device[1] == t)
+
+    def q_home(h):
+        return ((t * Hh + h) * C + out_r // T, lax.rem(out_r, T))
+
+    def q_source(s):
+        return (block_of(s), my_tp)
+
     def q_copy(h):
         return pltpu.make_async_remote_copy(
             src_ref=qs.at[h], dst_ref=qr.at[out_slot],
             send_sem=q_ss.at[h], recv_sem=q_rs.at[out_slot],
-            device_id=(h * R + out_r, t), device_id_type=MESH,
+            device_id=q_home(h), device_id_type=MESH,
         )
 
     def q_arrival(s):
         return pltpu.make_async_remote_copy(
             src_ref=qs.at[0], dst_ref=qr.at[s],
             send_sem=q_ss.at[0], recv_sem=q_rs.at[s],
-            device_id=(block_of(s), t), device_id_type=MESH,
+            device_id=q_source(s), device_id_type=MESH,
         )
 
     @pl.loop(0, Hh)
-    def _(h):
-        @pl.when(h * R + out_r != me)
+    def _(o):
+        h = lax.rem(me + o, Hh)
+
+        @pl.when(jnp.logical_not(is_me(q_home(h))))
         def _():
             q_copy(h).start()
 
-        @pl.when(h * R + out_r == me)
+        @pl.when(is_me(q_home(h)))
         def _():
             qr[out_slot] = qs[h]
+
+    loads[1].wait()
+    kvs[:, :HEAD_DIM] = head_norm(dot(wk[...], nrm[...], NT), kg).astype(jnp.bfloat16)
+    for h in range(Hh):
+        kvs[h, HEAD_DIM:KEY_ROWS] = gate_rows(h, -1.0, 0)
+    loads[2].wait()
+    kvs[:, KEY_ROWS:] = (
+        dot(wv[...], nrm[...], NT).astype(jnp.bfloat16).reshape(Hh, HEAD_DIM, L)
+    )
+
+    def kv_home(k):
+        return (t * span + k, relay)
+
+    def kv_copy(k):
+        return pltpu.make_async_remote_copy(
+            src_ref=kvs.at[k // C], dst_ref=kvr.at[me],
+            send_sem=kv_ss.at[k], recv_sem=kv_rs.at[me],
+            device_id=kv_home(k), device_id_type=MESH,
+        )
+
+    def kv_arrival(j, tp):
+        return pltpu.make_async_remote_copy(
+            src_ref=kvs.at[0], dst_ref=kvr.at[j],
+            send_sem=kv_ss.at[0], recv_sem=kv_rs.at[j],
+            device_id=(me, tp), device_id_type=MESH,
+        )
+
+    def kv_forward(j, o):
+        return pltpu.make_async_remote_copy(
+            src_ref=kvr.at[j], dst_ref=kvr.at[j],
+            send_sem=fw_ss.at[o - 1, j], recv_sem=kv_rs.at[j],
+            device_id=(me, lax.rem(t + o, T)), device_id_type=MESH,
+        )
+
+    @pl.loop(0, span)
+    def _(o):
+        k = lax.rem(me + o, span)
+
+        @pl.when(jnp.logical_not(is_me(kv_home(k))))
+        def _():
+            kv_copy(k).start()
+
+        @pl.when(is_me(kv_home(k)))
+        def _():
+            kvr[me] = kvs[k // C]
 
     loads[3].wait()
     pool_input = dot(nrm[...], wp[...], NT).astype(jnp.bfloat16)
@@ -205,78 +239,6 @@
     for c in pool_copies:
         c.start()
 
-    @pl.loop(1, n)
-    def _(o):
-        kv_arrival(o).wait_recv()
-
-    def scores(q_block, j):
-        return dot(kvr[j, :KEY_ROWS], q_block, TN)
-
-    def absorb(state, s, values):
-        top, den, acc = state
-        new_top = jnp.maximum(top, jnp.max(s, axis=0, keepdims=True))
-        old = jnp.exp(top - new_top)
-        w = jnp.exp(s - new_top)
-        den = den * old + jnp.sum(w, axis=0, keepdims=True)
-        acc = acc * old + dot(values, w.astype(jnp.bfloat16), NN)
-        return new_top, den, acc
-
-    allowed = lax.broadcasted_iota(jnp.int32, (L, L), 0) <= lax.broadcasted_iota(
-        jnp.int32, (L, L), 1
-    )
-
-    def at_copy(s):
-        return pltpu.make_async_remote_copy(
-            src_ref=att_s.at[s], dst_ref=attf.at[t, my_head],
-            send_sem=at_ss.at[s], recv_sem=at_rs.at[my_head],
-            device_id=(block_of(s), t), device_id_type=MESH,
-        )
-
-    def at_arrival(h):
-        return pltpu.make_async_remote_copy(
-            src_ref=att_s.at[0], dst_ref=attf.at[t, h],
-            send_sem=at_ss.at[0], recv_sem=at_rs.at[h],
-            device_id=(h * R + out_r, t), device_id_type=MESH,
-        )
-
-    @pl.loop(0, Hh)
-    def _(s):
-        b = block_of(s)
-
-        @pl.when(b != me)
-        def _():
-            q_arrival(s).wait_recv()
-
-        q_block = qr[s]
-        first = jnp.where(allowed, scores(q_block, b), masked_fill)
-        state = (
-            jnp.full((1, L), masked_fill, jnp.float32),
-            jnp.zeros((1, L), jnp.float32),
-            jnp.zeros((HEAD_DIM, L), jnp.float32),
-        )
-        state = absorb(state, first, kvr[b, KEY_ROWS:])
-
-        def single(j, state):
-            return absorb(state, scores(q_block, j), kvr[j, KEY_ROWS:])
-
-        def pair(p, state):
-            j = 2 * p
-            both = jnp.concatenate([scores(q_block, j), scores(q_block, j + 1)], axis=0)
-            values = jnp.concatenate([kvr[j, KEY_ROWS:], kvr[j + 1, KEY_ROWS:]], axis=1)
-            return absorb(state, both, values)
-
-        state = lax.fori_loop(0, b // 2, pair, state)
-        state = lax.fori_loop(2 * (b // 2), b, single, state)
-        att_s[s] = (state[2] / state[1]).astype(jnp.bfloat16)
-
-        @pl.when(b != me)
-        def _():
-            at_copy(s).start()
-
-        @pl.when(b == me)
-        def _():
-            attf[t, my_head] = att_s[s]
-
     for c in pool_copies:
         c.wait()
     loads[4].wait()
@@ -287,9 +249,102 @@
         else:
             total[...] += part
 
+    top[...] = jnp.full(top.shape, masked_fill, jnp.float32)
+    den[...] = jnp.zeros(den.shape, jnp.float32)
+    acc[...] = jnp.zeros(acc.shape, jnp.float32)
+    allowed = lax.broadcasted_iota(jnp.int32, (L, L), 0) <= lax.broadcasted_iota(
+        jnp.int32, (L, L), 1
+    )
+
+    @pl.loop(0, Hh)
+    def _(s):
+        @pl.when(jnp.logical_not(is_me(q_source(s))))
+        def _():
+            q_arrival(s).wait_recv()
+
+    def absorb(slots, j, masked):
+        logits = [dot(keys[...], qr[s], NN) for s in slots]
+        if masked:
+            logits = [jnp.where(allowed, x, masked_fill) for x in logits]
+        new = [jnp.maximum(top[s], jnp.max(x, axis=0, keepdims=True)) for s, x in zip(slots, logits)]
+        w = [jnp.exp(x - m) for x, m in zip(logits, new)]
+        parts = [dot(kvr[j, KEY_ROWS:], x.astype(jnp.bfloat16), NN) for x in w]
+        for s, m, x, part in zip(slots, new, w, parts):
+            old = jnp.exp(top[s] - m)
+            top[s] = m
+            den[s] = den[s] * old + jnp.sum(x, axis=0, keepdims=True)
+            acc[s] = acc[s] * old + part
+
+    def attend(j):
+        keys[...] = jnp.transpose(kvr[j, :KEY_ROWS])
+        p = lax.rem(j, 2 * R)
+        low = 2 * (j // (2 * R)) + jnp.where(p > my_r, 1, 0) + jnp.where(p > 2 * R - 1 - my_r, 1, 0)
+        diagonal = (p == my_r) | (p == 2 * R - 1 - my_r)
+
+        @pl.when(diagonal)
+        def _():
+            absorb([low], j, True)
+
+        low = low + jnp.where(diagonal, 1, 0)
+        pairs = (Hh - low) // 2
+
+        @pl.loop(0, pairs)
+        def _(i):
+            absorb([low + 2 * i, low + 2 * i + 1], j, False)
+
+        @pl.when(lax.rem(Hh - low, 2) == 1)
+        def _():
+            absorb([Hh - 1], j, False)
+
+    @pl.loop(0, span // T)
+    def _(step):
+        for u in range(T):
+            k = step * T + lax.rem(seat - t - u + 2 * T, T)
+            base = lax.rem(seat - k + span, span)
+            for m in range(T):
+                j = base + m * span
+
+                @pl.when(jnp.logical_not((u == 0) & is_me((j, my_tp))))
+                def _():
+                    kv_arrival(j, lax.rem(t + 1, T)).wait_recv()
+
+                if u == 0:
+                    for o in range(1, T):
+                        kv_forward(j, o).start()
+
+            @pl.loop(0, T)
+            def _(m):
+                attend(base + m * span)
+
+    def at_copy(s):
+        return pltpu.make_async_remote_copy(
+            src_ref=att_s.at[s], dst_ref=attf.at[my_tp, my_head],
+            send_sem=at_ss.at[s], recv_sem=at_rs.at[my_head],
+            device_id=q_source(s), device_id_type=MESH,
+        )
+
+    def at_arrival(h):
+        return pltpu.make_async_remote_copy(
+            src_ref=att_s.at[0], dst_ref=attf.at[t, h],
+            send_sem=at_ss.at[0], recv_sem=at_rs.at[h],
+            device_id=q_home(h), device_id_type=MESH,
+        )
+
+    @pl.loop(0, Hh)
+    def _(s):
+        att_s[s] = (acc[s] / den[s]).astype(jnp.bfloat16)
+
+        @pl.when(jnp.logical_not(is_me(q_source(s))))
+        def _():
+            at_copy(s).start()
+
+        @pl.when(is_me(q_source(s)))
+        def _():
+            attf[t, my_head] = att_s[s]
+
     @pl.loop(0, Hh)
     def _(h):
-        @pl.when(h * R + out_r != me)
+        @pl.when(jnp.logical_not(is_me(q_home(h))))
         def _():
             at_arrival(h).wait_recv()
 
@@ -308,17 +363,22 @@
         result = result + attn_part(lax.rem(t - o + T, T))
     out[...] = result.astype(jnp.bfloat16)
 
-    @pl.loop(1, n)
-    def _(o):
-        kv_copy(o).wait_send()
+    @pl.loop(0, span)
+    def _(k):
+        @pl.when(jnp.logical_not(is_me(kv_home(k))))
+        def _():
+            kv_copy(k).wait_send()
+
+        for o in range(1, T):
+            kv_forward(k * T + t, o).wait_send()
 
     @pl.loop(0, Hh)
     def _(h):
-        @pl.when(h * R + out_r != me)
+        @pl.when(jnp.logical_not(is_me(q_home(h))))
         def _():
             q_copy(h).wait_send()
 
-        @pl.when(block_of(h) != me)
+        @pl.when(jnp.logical_not(is_me(q_source(h))))
         def _():
             at_copy(h).wait_send()
 
@@ -364,9 +424,13 @@
                 pltpu.VMEM((Hh, HEAD_DIM, L), bf),
                 pltpu.VMEM((T, Hh, HEAD_DIM, L), bf),
                 pltpu.VMEM((L, Dt), f32),
+                pltpu.VMEM((L, KEY_ROWS), bf),
+                pltpu.VMEM((Hh, 1, L), f32),
+                pltpu.VMEM((Hh, 1, L), f32),
+                pltpu.VMEM((Hh, HEAD_DIM, L), f32),
                 dma((6,)),
                 dma((S,)), dma((S,)),
-                dma((n - 1,)), dma((n - 1,)),
+                dma((n // T,)), dma((n,)), dma((S, n)),
                 dma((Hh,)), dma((Hh,)),
                 dma, dma,
                 dma((S,)), dma((S,)),
@@ -378,7 +442,7 @@
             ),
         )(
             tokens, norm_gain.reshape(1, -1), query_weight, key_weight, value_weight,
-            pool_weight, query_gain.reshape(-1, 1), key_gain.reshape(-1, 1), cum_gate.T,
+            pool_weight, query_gain.reshape(1, -1), key_gain.reshape(1, -1), cum_gate.T,
             out_pool_weight, out_attn_weight,
         )
 

time: 75.4 us -> 64.2 us (0.85)
  the two profiles are of different devices: /device:TPU:31 before, /device:TPU:0 now
where the time goes in v2:
time: 64.2 us; the launch traced here: 64 us
  Pallas kernels  62.1 us (97%)
  local copies, waits for them, and re-layouts  1.87 us (3%)
    pallas_call x1, Pallas kernels, per_device(): pl.pallas_call(functools.partial(kernel, n, T, R, Hh), out_shape=jax.Shap...  62.1 us
    unnamed x1, local copies, waits for them, and re-layouts  1.87 us

profile of v2, /device:TPU:0, one launch (start us, length us, event | category | flops | bytes accessed | tf_op | source)
XLA Modules:
  0.0 64.0 jit_solution(8122926473266617207)
XLA Ops:
  0.0 62.1 %shard_map.109 = bf16[256,1024]{1,0:T(8,128)(2,1)} custom-call(bf16[256,1024]{1,0:T(8,128)(2,1)} %tok.1, f32[1,2048]{1,0:T(1,128)} %bitcast.4, bf16[512,2048]{1,0:T(8,128)(2,1)} %wq_h.1, bf16[512,2048]{1,0:T(8,128)(2,1)} %wk_h.1, bf16[512,2048]{1,0:T(8,128)(2,1)} %wv_h.1, bf16[512,2048]{1,0:T(8,128)(2,1)} %wp_h.1, f32[1,64]{1,0:T(1,128)} %bitcast.6, ...), custom_call_target="tpu_custom_call" | custom-call | tf_op jit(solution)/shard_map/pallas_call | solution.py:403
  62.1 1.9 %copy.13 = bf16[256,1024]{1,0:T(8,128)(2,1)} copy(bf16[256,1024]{1,0:T(8,128)(2,1)} %shard_map.109) | data formatting | bytes 1048576

commit v3 on v2

--- a/solution.py
+++ b/solution.py
@@ -262,39 +262,59 @@
         def _():
             q_arrival(s).wait_recv()
 
-    def absorb(slots, j, masked):
-        logits = [dot(keys[...], qr[s], NN) for s in slots]
+    def absorb(work, masked):
+        logits = [dot(keys[m], qr[s], NN) for s, m, j in work]
         if masked:
             logits = [jnp.where(allowed, x, masked_fill) for x in logits]
+        slots = [s for s, m, j in work]
         new = [jnp.maximum(top[s], jnp.max(x, axis=0, keepdims=True)) for s, x in zip(slots, logits)]
         w = [jnp.exp(x - m) for x, m in zip(logits, new)]
-        parts = [dot(kvr[j, KEY_ROWS:], x.astype(jnp.bfloat16), NN) for x in w]
+        parts = [
+            dot(kvr[j, KEY_ROWS:], x.astype(jnp.bfloat16), NN) for (s, m, j), x in zip(work, w)
+        ]
         for s, m, x, part in zip(slots, new, w, parts):
             old = jnp.exp(top[s] - m)
             top[s] = m
             den[s] = den[s] * old + jnp.sum(x, axis=0, keepdims=True)
             acc[s] = acc[s] * old + part
 
-    def attend(j):
-        keys[...] = jnp.transpose(kvr[j, :KEY_ROWS])
+    def attend_halves(j):
+        half = Hh // 2
+        for m in range(2):
+            keys[m] = jnp.transpose(kvr[j + m * span, :KEY_ROWS])
         p = lax.rem(j, 2 * R)
         low = 2 * (j // (2 * R)) + jnp.where(p > my_r, 1, 0) + jnp.where(p > 2 * R - 1 - my_r, 1, 0)
         diagonal = (p == my_r) | (p == 2 * R - 1 - my_r)
+        absorb([(s, 0, j) for s in range(half, Hh)], False)
 
         @pl.when(diagonal)
         def _():
-            absorb([low], j, True)
+            absorb([(low, 0, j), (low + half, 1, j + span)], True)
+
+        @pl.loop(low + jnp.where(diagonal, 1, 0), half)
+        def _(s):
+            absorb([(s, 0, j), (s + half, 1, j + span)], False)
+
+    def attend(j):
+        keys[0] = jnp.transpose(kvr[j, :KEY_ROWS])
+        p = lax.rem(j, 2 * R)
+        low = 2 * (j // (2 * R)) + jnp.where(p > my_r, 1, 0) + jnp.where(p > 2 * R - 1 - my_r, 1, 0)
+        diagonal = (p == my_r) | (p == 2 * R - 1 - my_r)
+
+        @pl.when(diagonal)
+        def _():
+            absorb([(low, 0, j)], True)
 
         low = low + jnp.where(diagonal, 1, 0)
         pairs = (Hh - low) // 2
 
         @pl.loop(0, pairs)
         def _(i):
-            absorb([low + 2 * i, low + 2 * i + 1], j, False)
+            absorb([(low + 2 * i, 0, j), (low + 2 * i + 1, 0, j)], False)
 
         @pl.when(lax.rem(Hh - low, 2) == 1)
         def _():
-            absorb([Hh - 1], j, False)
+            absorb([(Hh - 1, 0, j)], False)
 
     @pl.loop(0, span // T)
     def _(step):
@@ -312,9 +332,13 @@
                     for o in range(1, T):
                         kv_forward(j, o).start()
 
-            @pl.loop(0, T)
-            def _(m):
-                attend(base + m * span)
+            if T == 2 and span % (2 * R) == 0:
+                attend_halves(base)
+            else:
+
+                @pl.loop(0, T)
+                def _(m):
+                    attend(base + m * span)
 
     def at_copy(s):
         return pltpu.make_async_remote_copy(
@@ -424,7 +448,7 @@
                 pltpu.VMEM((Hh, HEAD_DIM, L), bf),
                 pltpu.VMEM((T, Hh, HEAD_DIM, L), bf),
                 pltpu.VMEM((L, Dt), f32),
-                pltpu.VMEM((L, KEY_ROWS), bf),
+                pltpu.VMEM((2, L, KEY_ROWS), bf),
                 pltpu.VMEM((Hh, 1, L), f32),
                 pltpu.VMEM((Hh, 1, L), f32),
                 pltpu.VMEM((Hh, HEAD_DIM, L), f32),

time: 64.2 us -> 57.8 us (0.900)
  Pallas kernels: 62.1 us -> 55.7 us
    pallas_call x1, Pallas kernels: 62.1 us -> 55.7 us  [per_device(): pl.pallas_call(functools.partial(kernel, n, T, R, Hh), out_shape=jax.Shap...]
where the time goes in v3:
time: 57.8 us; the launch traced here: 57.6 us
  Pallas kernels  55.7 us (96%)
  local copies, waits for them, and re-layouts  1.87 us (3%)
    pallas_call x1, Pallas kernels, per_device(): pl.pallas_call(functools.partial(kernel, n, T, R, Hh), out_shape=jax.Shap...  55.7 us
    unnamed x1, local copies, waits for them, and re-layouts  1.87 us

profile of v3, /device:TPU:0, one launch (start us, length us, event | category | flops | bytes accessed | tf_op | source)
XLA Modules:
  0.0 57.6 jit_solution(12272049118052809892)
XLA Ops:
  0.0 55.7 %shard_map.109 = bf16[256,1024]{1,0:T(8,128)(2,1)} custom-call(bf16[256,1024]{1,0:T(8,128)(2,1)} %tok.1, f32[1,2048]{1,0:T(1,128)} %bitcast.4, bf16[512,2048]{1,0:T(8,128)(2,1)} %wq_h.1, bf16[512,2048]{1,0:T(8,128)(2,1)} %wk_h.1, bf16[512,2048]{1,0:T(8,128)(2,1)} %wv_h.1, bf16[512,2048]{1,0:T(8,128)(2,1)} %wp_h.1, f32[1,64]{1,0:T(1,128)} %bitcast.6, ...), custom_call_target="tpu_custom_call" | custom-call | tf_op jit(solution)/shard_map/pallas_call | solution.py:427
  55.7 1.9 %copy.13 = bf16[256,1024]{1,0:T(8,128)(2,1)} copy(bf16[256,1024]{1,0:T(8,128)(2,1)} %shard_map.109) | data formatting | bytes 1048576

commit v4 on v3

--- a/solution.py
+++ b/solution.py
@@ -89,13 +89,12 @@
     for c in tok_copies:
         c.start()
     tokf[t] = tok[...]
-    for c in tok_copies:
-        c.wait()
-
     Dt = tok.shape[1]
-    square = jnp.zeros((L, 1), jnp.float32)
-    for i in range(T):
-        x = tokf[i].astype(jnp.float32)
+    x = tok[...].astype(jnp.float32)
+    square = jnp.sum(x * x, axis=-1, keepdims=True)
+    for o in range(1, T):
+        tok_copies[o - 1].wait()
+        x = tokf[lax.rem(t - o + T, T)].astype(jnp.float32)
         square += jnp.sum(x * x, axis=-1, keepdims=True)
     scale = lax.rsqrt(square / (T * Dt) + epsilon)
     for i in range(T):

time: 57.8 us -> 57.8 us (level)
  no operation moved by 1% of the time
where the time goes in v4:
time: 57.8 us; the launch traced here: 57.6 us
  Pallas kernels  55.7 us (96%)
  local copies, waits for them, and re-layouts  1.87 us (3%)
    pallas_call x1, Pallas kernels, per_device(): pl.pallas_call(functools.partial(kernel, n, T, R, Hh), out_shape=jax.Shap...  55.7 us
    unnamed x1, local copies, waits for them, and re-layouts  1.87 us

profile of v4, /device:TPU:0, one launch (start us, length us, event | category | flops | bytes accessed | tf_op | source)
XLA Modules:
  0.0 57.6 jit_solution(5462970793167151352)
XLA Ops:
  0.0 55.7 %shard_map.109 = bf16[256,1024]{1,0:T(8,128)(2,1)} custom-call(bf16[256,1024]{1,0:T(8,128)(2,1)} %tok.1, f32[1,2048]{1,0:T(1,128)} %bitcast.4, bf16[512,2048]{1,0:T(8,128)(2,1)} %wq_h.1, bf16[512,2048]{1,0:T(8,128)(2,1)} %wk_h.1, bf16[512,2048]{1,0:T(8,128)(2,1)} %wv_h.1, bf16[512,2048]{1,0:T(8,128)(2,1)} %wp_h.1, f32[1,64]{1,0:T(1,128)} %bitcast.6, ...), custom_call_target="tpu_custom_call" | custom-call | tf_op jit(solution)/shard_map/pallas_call | solution.py:426
  55.7 1.9 %copy.13 = bf16[256,1024]{1,0:T(8,128)(2,1)} copy(bf16[256,1024]{1,0:T(8,128)(2,1)} %shard_map.109) | data formatting | bytes 1048576
